TPU v7x, 32 devices: a whole 2x2x4 slice. The times are simulated.
32 devices in a mesh: kv: 8 (over z, y), tp: 4 (over x, core).
Axes of the slice: x: 2, y: 2, z: 4, core: 2. Of those that a mesh axis runs over, the one named last changes fastest.
Arguments:
- residual_entries: bfloat16 [512, 4096], P(None, ('kv', 'tp')), may hold values from -6 to 6
- fresh_extents: int32 [64], replicated, may hold values from 1 to 8, 256 in all
- memory_matrix: float32 [64, 16, 128, 128], P('kv', 'tp'), may hold values from -3 to 3
- initial_rescale_vector: float32 [4096], P('kv'), may hold values from 0.1 to 1.9
- probe_matrix: bfloat16 [4096, 2048], P('kv', 'tp'), may hold values from -0.09375 to 0.09375
- retain_matrix: bfloat16 [4096, 2048], P('kv', 'tp'), may hold values from -0.09375 to 0.09375
- content_matrix: bfloat16 [4096, 2048], P('kv', 'tp'), may hold values from -0.09375 to 0.09375
- result_switch_matrix: bfloat16 [4096, 2048], P('kv', 'tp'), may hold values from -0.09375 to 0.09375
- retain_lower_limit: float32 [2048], P('tp'), may hold values from 0 to 0.9
- extra_shrink_log: float32 [512, 16], P('kv', 'tp'), may hold values from -0.7 to 0
- lane_result_rescale: float32 [128], replicated, may hold values from 0.1 to 1.9
- result_matrix: bfloat16 [2048, 4096], P('tp', 'kv'), may hold values from -0.125 to 0.125
- later_rescale_vector: float32 [4096], P(('kv', 'tp')), may hold values from 0.1 to 1.9
- mixer_switch_matrix: bfloat16 [4096, 11008], P(None, ('kv', 'tp')), may hold values from -0.09375 to 0.09375
- widening_matrix: bfloat16 [4096, 11008], P(None, ('kv', 'tp')), may hold values from -0.09375 to 0.09375
- narrowing_matrix: bfloat16 [11008, 4096], P(('kv', 'tp')), may hold values from -0.109375 to 0.109375
Outputs:
- mixed: bfloat16 [512, 4096], P(None, ('kv', 'tp'))
- new_state: float32 [64, 16, 128, 128], P('kv', 'tp')
Inputs may be any that keep to these rules, and one draw needn't show every extreme that they name: `fresh_extents`: the lengths sum to exactly 256.
All inputs are finite; a program needn't handle non-finite values.
Results may differ from a plain program's by a relative error of at most 0.022.
Values may be sent and summed in bfloat16 or wider, within the bound.
A program may use at most 64 MiB of HBM per device.

v0:
```python
import jax
import jax.numpy as jnp
from jax import lax
from jax.sharding import PartitionSpec as P

D = 4096
HEAD = 128
FRESH_PLACES = 8


epsilon = 1e-06


def local(
    residual_entries,
    fresh_extents,
    memory_matrix,
    initial_rescale_vector,
    probe_matrix,
    retain_matrix,
    content_matrix,
    result_switch_matrix,
    retain_lower_limit,
    extra_shrink_log,
    lane_result_rescale,
    result_matrix,
    later_rescale_vector,
    mixer_switch_matrix,
    widening_matrix,
    narrowing_matrix,
):
    sequences_per_device = memory_matrix.shape[0]
    heads_per_device = memory_matrix.shape[1]
    rows_dev = sequences_per_device * FRESH_PLACES
    all_rows = residual_entries.shape[0]
    kv_index = lax.axis_index("kv")
    tokens_wide = residual_entries.astype(jnp.float32)
    columns = lax.all_gather(residual_entries, "tp", axis=1, tiled=True)
    squares = lax.psum(jnp.sum(tokens_wide * tokens_wide, axis=1), ("kv", "tp"))
    own_squares = lax.dynamic_slice_in_dim(squares, kv_index * rows_dev, rows_dev)
    first_scale = lax.rsqrt(own_squares / D + epsilon)
    scaled = (columns.astype(jnp.float32) * initial_rescale_vector).astype(jnp.bfloat16)
    projected = (
        lax.psum_scatter(
            jnp.concatenate(
                [
                    jnp.dot(scaled, weight, preferred_element_type=jnp.float32)
                    for weight in (
                        probe_matrix,
                        retain_matrix,
                        content_matrix,
                        result_switch_matrix,
                    )
                ],
                axis=1,
            ).astype(jnp.bfloat16),
            "kv",
            scatter_dimension=0,
            tiled=True,
        ).astype(jnp.float32)
        * first_scale[:, None]
    )
    width_dev = probe_matrix.shape[1]
    shape_four = (sequences_per_device, FRESH_PLACES, heads_per_device, HEAD)
    z_query = projected[:, :width_dev]
    z_forget = projected[:, width_dev : 2 * width_dev].reshape(shape_four)
    z_input = projected[:, 2 * width_dev : 3 * width_dev].reshape(shape_four)
    z_outgate = projected[:, 3 * width_dev :]
    own_lengths = lax.dynamic_slice_in_dim(
        fresh_extents, kv_index * sequences_per_device, sequences_per_device
    )
    living = jnp.arange(FRESH_PLACES, dtype=jnp.int32)[None, :] < own_lengths[:, None]
    query = jax.nn.silu(z_query).reshape(shape_four)
    bounds = retain_lower_limit.reshape(heads_per_device, HEAD)
    retain_factor = bounds + (1.0 - bounds) * jax.nn.sigmoid(z_forget)
    shrink_exponent = jnp.log(retain_factor) + extra_shrink_log.reshape(
        sequences_per_device, FRESH_PLACES, heads_per_device, 1
    )
    decays = jnp.where(living[:, :, None, None], jnp.exp(shrink_exponent), 1.0)
    key_gate = jnp.where(living[:, :, None, None], 1.0 - retain_factor, 0.0)
    carried = memory_matrix
    outputs = []
    for position in range(FRESH_PLACES):
        carried = (
            decays[:, position, :, :, None] * carried
            + key_gate[:, position, :, :, None] * z_input[:, position, :, None, :]
        )
        outputs.append(
            jnp.einsum(
                "bhd,bhdv->bhv", query[:, position], carried, precision=lax.Precision.HIGHEST
            )
        )
    heads_out = jnp.stack(outputs, axis=1)
    heads_out = (
        heads_out
        * lax.rsqrt(jnp.mean(heads_out * heads_out, axis=-1, keepdims=True) + epsilon)
        * lane_result_rescale
    )
    normed = jnp.where(
        living.reshape(rows_dev)[:, None],
        heads_out.reshape(rows_dev, width_dev) * jax.nn.silu(z_outgate),
        0.0,
    ).astype(jnp.bfloat16)
    head_partial = jnp.dot(
        lax.all_gather(normed, "kv", axis=0, tiled=True),
        result_matrix,
        preferred_element_type=jnp.float32,
    ).astype(jnp.bfloat16)
    attended = lax.psum_scatter(head_partial, "tp", scatter_dimension=1, tiled=True).astype(
        jnp.float32
    )
    residual = (tokens_wide + attended).astype(jnp.bfloat16)
    resid_wide = residual.astype(jnp.float32)
    resid_squares = lax.psum(jnp.sum(resid_wide * resid_wide, axis=1), ("kv", "tp"))
    second_in = (
        resid_wide * later_rescale_vector * lax.rsqrt(resid_squares / D + epsilon)[:, None]
    ).astype(jnp.bfloat16)
    live_rows = (
        jnp.arange(FRESH_PLACES, dtype=jnp.int32)[None, :] < fresh_extents[:, None]
    ).reshape(all_rows)
    live_order = jnp.argsort(1 - live_rows.astype(jnp.int32), stable=True)[: all_rows // 2]
    mixer_input = jnp.take(second_in, live_order, axis=0)
    piece = lax.all_gather(mixer_input, ("kv", "tp"), axis=1, tiled=True)
    gated = jnp.dot(piece, mixer_switch_matrix, preferred_element_type=jnp.float32)
    upward = jnp.dot(piece, widening_matrix, preferred_element_type=jnp.float32)
    hidden = (jax.nn.silu(gated) * upward).astype(jnp.bfloat16)
    mixer_terms = lax.psum_scatter(
        jnp.dot(hidden, narrowing_matrix, preferred_element_type=jnp.float32),
        ("kv", "tp"),
        scatter_dimension=1,
        tiled=True,
    )
    down_terms = (
        jnp.zeros((all_rows, mixer_terms.shape[1]), jnp.float32).at[live_order].set(mixer_terms)
    )
    mixed = jnp.where(live_rows[:, None], resid_wide + down_terms, 0.0).astype(jnp.bfloat16)
    return (mixed, carried)


def solution(mesh):
    placed = (
        P(None, ("kv", "tp")),
        P(),
        P("kv", "tp", None, None),
        P("kv"),
        P("kv", "tp"),
        P("kv", "tp"),
        P("kv", "tp"),
        P("kv", "tp"),
        P("tp"),
        P("kv", "tp"),
        P(),
        P("tp", "kv"),
        P(("kv", "tp")),
        P(None, ("kv", "tp")),
        P(None, ("kv", "tp")),
        P(("kv", "tp"), None),
    )
    return jax.shard_map(
        local,
        mesh=mesh,
        in_specs=placed,
        out_specs=(P(None, ("kv", "tp")), P("kv", "tp", None, None)),
        check_vma=False,
    )
```

profile of v0, /device:TPU:0, one launch (start us, length us, event | category | flops | bytes accessed | tf_op | source)
XLA Modules:
  0.0 449.1 jit_solution(15715938203859313457)
XLA Ops:
  7.3 9.0 %all_gather.9 = bf16[512,512]{1,0:T(8,128)(2,1)S(1)} all-gather(bf16[512,128]{1,0:T(8,128)(2,1)} %param.16), channel_id=1, replica_groups=mesh['kv'=8,'tp'=4] {'tp'}, dimensions={1}, use_global_device_ids=true | all-gather | bytes 655360 | tf_op jit(solution)/shard_map/all_gather | solution.py:38
  16.3 1.6 convolution_convert_fusion.3
  19.4 1.5 pad_maximum_fusion
  20.8 4.0 copy.203
  26.0 40.8 %psum.14 = f32[512]{0:T(512)S(1)} all-reduce(f32[512]{0:T(512)S(1)} %fusion.25), channel_id=1, replica_groups=mesh['kv'=8,'tp'=4] {'kv','tp'}, use_global_device_ids=true, to_apply=%region_2.0 | all-reduce | flops 512 | bytes 4096 | tf_op jit(solution)/shard_map/psum | solution.py:39
  66.8 28.5 %reduce-scatter.10.cloned.1.call-done = bf16[64,2048]{1,0:T(8,128)(2,1)} async-done(((bf16[512,2048]{1,0:T(8,128)(2,1)}), bf16[64,2048]{1,0:T(8,128)(2,1)}) %reduce-scatter.10.cloned.1.call-update) | async-done | bytes 262160 | tf_op jit(solution)/shard_map/reduce_scatter | solution.py:44
  97.3 2.8 fusion
  100.1 4.3 fusion.18
  104.4 6.1 %fusion.1 = f32[8,4,1,128]{3,2,1,0:T(1,128)S(1)} fusion(f32[8,4,128]{2,1,0:T(4,128)S(1)} %bitcast.159, f32[8,4,128]{2,1,0:T(4,128)S(1)} %bitcast.183, f32[8,4,128]{2,1,0:T(4,128)S(1)} %bitcast.175, f32[8,4,128,128]{3,2,1,0:T(8,128)S(1)} %copy-done.1, f32[8,4,128]{2,1,0:T(4,128)S(1)} %bitcast.157, f32[8,4,128]{2,1,0:T(4,128)S(1)} %bitcast.181, ...), kind=kOutput, calls=%fused_computation.12 | convolution fusion | flops 11010048 | bytes 2277376 | tf_op jit(solution)/shard_map/bhd,bhdv->bhv/dot_general | solution.py:89
  110.5 9.0 %multiply_add_fusion = (f32[8,4,128,128]{3,2,1,0:T(8,128)S(1)}, f32[8,4,128,128]{3,2,1,0:T(8,128)S(1)}) fusion(f32[8,4,128]{2,1,0:T(4,128)S(1)} %bitcast.161, f32[8,4,128]{2,1,0:T(4,128)S(1)} %bitcast.185, f32[8,4,128]{2,1,0:T(4,128)S(1)} %bitcast.174, f32[8,4,128]{2,1,0:T(4,128)S(1)} %bitcast.154, f32[8,4,128]{2,1,0:T(4,128)S(1)} %bitcast.171, ...), kind=kLoop, calls=%fused_computation.3 | loop fusion | flops 12582912 | bytes 6684672 | tf_op jit(solution)/shard_map/add | solution.py:85
  119.5 6.1 %fusion.3 = f32[8,4,1,128]{3,2,1,0:T(1,128)S(1)} fusion(f32[8,4,128]{2,1,0:T(4,128)S(1)} %bitcast.155, f32[8,4,128]{2,1,0:T(4,128)S(1)} %bitcast.172, f32[8,4,128]{2,1,0:T(4,128)S(1)} %bitcast.170, f32[8,4,128,128]{3,2,1,0:T(8,128)S(1)} %get-tuple-element.5, f32[8,4,128]{2,1,0:T(4,128)S(1)} %bitcast.152, f32[8,4,128]{2,1,0:T(4,128)S(1)} %bitcast.167, ...), kind=kOutput, calls=%fused_computation.14 | convolution fusion | flops 11010048 | bytes 2277376 | tf_op jit(solution)/shard_map/bhd,bhdv->bhv/dot_general | solution.py:89
  125.6 4.3 fusion.19
  129.8 3.0 fusion.2
  132.8 1.9 fusion.49
  134.7 1.9 fusion.44
  137.0 31.3 %all_gather.10 = bf16[512,512]{1,0:T(8,128)(2,1)S(1)} all-gather(bf16[64,512]{1,0:T(8,128)(2,1)S(1)} %fusion.41), channel_id=1, replica_groups=mesh['kv'=8,'tp'=4] {'kv'}, dimensions={0}, use_global_device_ids=true | all-gather | bytes 589824 | tf_op jit(solution)/shard_map/all_gather | solution.py:105
  170.0 3.8 sort.17
  173.8 16.7 %reduce-scatter.12.cloned.1.call-done = bf16[128,512]{1,0:T(8,128)(2,1)} async-done(((bf16[512,512]{1,0:T(8,128)(2,1)}), bf16[128,512]{1,0:T(8,128)(2,1)}) %reduce-scatter.12.cloned.1.call-update) | async-done | bytes 131088
  191.7 39.3 %psum.15 = f32[512]{0:T(512)S(1)} all-reduce(f32[512]{0:T(512)S(1)} %fusion.29), channel_id=1, replica_groups=mesh['kv'=8,'tp'=4] {'kv','tp'}, use_global_device_ids=true, to_apply=%region_7.8 | all-reduce | flops 512 | bytes 4096 | tf_op jit(solution)/shard_map/psum | solution.py:114
  232.9 53.8 %all-gather.2.cloned.1.call-done = bf16[256,4096]{1,0:T(8,128)(2,1)} async-done(((bf16[256,128]{1,0:T(8,128)(2,1)}), bf16[256,4096]{1,0:T(8,128)(2,1)}) %all-gather.2.cloned.1.call-update) | async-done | bytes 2097168 | tf_op jit(solution)/shard_map/all_gather | solution.py:123
  286.7 3.4 fusion.59
  290.1 8.0 %fusion.5 = f32[256,4096]{1,0:T(8,128)} fusion(bf16[344,4096]{1,0:T(8,128)(2,1)S(1)} %copy-done, bf16[256,4096]{1,0:T(8,128)(2,1)} %all-gather.2.cloned.1.call-done, bf16[4096,344]{0,1:T(8,128)(2,1)} %param.30, f32[256,344]{0,1:T(8,128)S(1)} %fusion.59), kind=kOutput, calls=%fused_computation.22 | convolution fusion | flops 1443368960 | bytes 12279808 | tf_op jit(solution)/shard_map/dot_general | solution.py:128
  298.1 142.1 %reduce-scatter.8.cloned.1.call-done = f32[256,128]{1,0:T(8,128)} async-done(((f32[256,4096]{1,0:T(8,128)}), f32[256,128]{1,0:T(8,128)}) %reduce-scatter.8.cloned.1.call-update) | async-done | bytes 131088 | tf_op jit(solution)/shard_map/reduce_scatter | solution.py:127
  440.2 1.6 scatter_custom_fusion
  (89 shorter events, 10.4 us)
Async XLA Ops:
  7.2 282.9 %copy-start = (bf16[344,4096]{1,0:T(8,128)(2,1)S(1)}, bf16[344,4096]{1,0:T(8,128)(2,1)}, u32[]{:S(2)}) copy-start(bf16[344,4096]{1,0:T(8,128)(2,1)} %param.31) | copy-start | bytes 8454148
  7.2 10.7 %copy-start.13 = (f32[512]{0:T(512)S(1)}, f32[512]{0:T(512)}, u32[]{:S(2)}) copy-start(f32[512]{0:T(512)} %param.19) | copy-start | bytes 6148
  7.2 10.7 %copy-start.10 = (bf16[512,512]{1,0:T(8,128)(2,1)S(1)}, bf16[512,512]{1,0:T(8,128)(2,1)}, u32[]{:S(2)}) copy-start(bf16[512,512]{1,0:T(8,128)(2,1)} %param.22) | copy-start | bytes 1572868
  7.2 88.1 %reduce-scatter.10.cloned.1.call-start = ((), (), s32[]{:S(2)}) async-start(), calls=%async_computation.5 | async-start | bytes 2359296 | tf_op jit(solution)/shard_map/reduce_scatter | solution.py:44
  7.2 11.1 %copy-start.11 = (bf16[512,512]{1,0:T(8,128)(2,1)S(1)}, bf16[512,512]{1,0:T(8,128)(2,1)}, u32[]{:S(2)}) copy-start(bf16[512,512]{1,0:T(8,128)(2,1)} %param.23) | copy-start | bytes 1572868
  16.3 2.6 copy-start.12
  24.8 0.7 copy-start.9
  24.8 0.9 copy-start.6
  24.8 1.0 copy-start.3
  24.8 42.0 %copy-start.8 = (f32[128]{0:T(128)S(1)}, f32[128]{0:T(128)}, u32[]{:S(2)}) copy-start(f32[128]{0:T(128)} %param.26) | copy-start | bytes 1540
  24.8 42.0 %copy-start.5 = (f32[512]{0:T(512)S(1)}, f32[512]{0:T(512)}, u32[]{:S(2)}) copy-start(f32[512]{0:T(512)} %param.24) | copy-start | bytes 6148
  24.9 165.7 %reduce-scatter.12.cloned.1.call-start = ((), (), s32[]{:S(2)}) async-start(), calls=%async_computation.6 | async-start | bytes 655360
  95.3 2.0 copy-start.1
  119.5 15.3 %copy-start.2 = (f32[8,4,128,128]{3,2,1,0:T(8,128)}, f32[8,4,128,128]{3,2,1,0:T(8,128)S(1)}, u32[]{:S(2)}) copy-start(f32[8,4,128,128]{3,2,1,0:T(8,128)S(1)} %get-tuple-element.4) | copy-start | bytes 6291460
  134.7 33.6 %copy-start.4 = (bf16[512,512]{1,0:T(8,128)(2,1)S(1)}, bf16[512,512]{1,0:T(8,128)(2,1)}, u32[]{:S(2)}) copy-start(bf16[512,512]{1,0:T(8,128)(2,1)} %param.27) | copy-start | bytes 1572868
  137.0 94.1 %copy-start.7 = (f32[128]{0:T(128)S(1)}, f32[128]{0:T(128)}, u32[]{:S(2)}) copy-start(f32[128]{0:T(128)} %param.28) | copy-start | bytes 1540
  169.8 116.9 %all-gather.2.cloned.1.call-start = ((), (), s32[]{:S(2)}) async-start(), calls=%async_computation.3 | async-start | bytes 2162688 | tf_op jit(solution)/shard_map/all_gather | solution.py:123
  232.8 207.4 %reduce-scatter.8.cloned.1.call-start = ((), (), s32[]{:S(2)}) async-start(), calls=%async_computation.4 | async-start | bytes 4325376 | tf_op jit(solution)/shard_map/reduce_scatter | solution.py:127
Sparse Core Ops, SparseCore 0:
  25.0 70.2 reduce-scatter.9
  169.9 20.6 reduce-scatter.11
  232.9 53.6 all-gather.1
  298.2 141.9 reduce-scatter.7
where the time goes:
time: 449 us
  waiting for transfers between devices  241 us (54%)
  blocking collectives  120 us (27%)
  matrix products  45.2 us (10%)
  other arithmetic  18.2 us (4%)
  between operations  14.2 us (3%)
  local copies, waits for them, and re-layouts  9.9 us (2%)
    reduce_scatter x1, waiting for transfers between devices, local(): lax.psum_scatter(jnp.dot(hidden, narrowing_matrix, preferred_element_type...  142 us
    all_gather x1, waiting for transfers between devices, local(): piece = lax.all_gather(mixer_input, ('kv', 'tp'), axis=1, tiled=True)  53.8 us
    psum x1, blocking collectives, local(): squares = lax.psum(jnp.sum(tokens_wide * tokens_wide, axis=1), ('kv', 'tp'))  40.8 us
    psum x1, blocking collectives, local(): lax.psum(jnp.sum(resid_wide * resid_wide, axis=1), ('kv', 'tp'))  39.3 us
    all_gather x1, blocking collectives, local(): lax.all_gather(normed, 'kv', axis=0, tiled=True)  31.3 us
    dot_general x8, matrix products, local(): jnp.einsum('bhd,bhdv->bhv', query[:, position], carried, precision=lax.Pr...  30.3 us
    reduce_scatter x1, waiting for transfers between devices, local(): lax.psum_scatter(jnp.concatenate([jnp.dot(scaled, weight, preferred_eleme...  28.5 us
    unnamed x5, waiting for transfers between devices  16.8 us
  transfers between devices with their start and end apart: 4, of which 4 were waited for; matrix products, arithmetic and copies ran while one was open for 1% of the time, Pallas kernels for 0%

commit v1 on v0

--- a/solution.py
+++ b/solution.py
@@ -1,17 +1,603 @@
+import functools
+
 import jax
 import jax.numpy as jnp
 from jax import lax
+from jax.experimental import pallas as pl
+from jax.experimental.pallas import tpu as pltpu
 from jax.sharding import PartitionSpec as P
 
-D = 4096
-HEAD = 128
 FRESH_PLACES = 8
-
-
+CORES = 2
 epsilon = 1e-06
 
+F32, BF16 = jnp.float32, jnp.bfloat16
+VM = pl.BlockSpec(memory_space=pltpu.VMEM)
+HBM = pl.BlockSpec(memory_space=pl.ANY)
+LIMIT = 60 * 1024 * 1024
+
+
+class Place:
+    def __init__(self, kv_size, tp_size):
+        self.sizes = {
+            "z": 4 if kv_size % 4 == 0 else kv_size,
+            "y": kv_size // 4 if kv_size % 4 == 0 else 1,
+            "x": tp_size // CORES,
+            "c": CORES,
+        }
+        kv, tp = lax.axis_index("kv"), lax.axis_index("tp")
+        width = self.sizes["y"]
+        self.at = {"z": kv // width, "y": kv % width, "x": tp // CORES, "c": tp % CORES}
+
+    def partner(self, axis, step):
+        return (self.at[axis] + step) % self.sizes[axis]
+
+    def device(self, **moved):
+        at = {**self.at, **moved}
+        return (at["z"] * self.sizes["y"] + at["y"], at["x"] * CORES + at["c"])
+
+
+def greet(devices):
+    barrier = pltpu.get_barrier_semaphore()
+    for device in devices:
+        pl.semaphore_signal(
+            barrier, inc=1, device_id=device, device_id_type=pl.DeviceIdType.MESH
+        )
+    pl.semaphore_wait(barrier, len(devices))
+
+
+def along(place, axes):
+    return [
+        place.device(**{axis: place.partner(axis, step)})
+        for axis in axes
+        for step in range(1, place.sizes[axis])
+    ]
+
+
+class Sender:
+    def __init__(self, send_sems, recv_sems):
+        self.send_sems, self.recv_sems, self.used, self.copies = send_sems, recv_sems, 0, []
+
+    def start(self, source, target, device):
+        copy = pltpu.make_async_remote_copy(
+            src_ref=source,
+            dst_ref=target,
+            send_sem=self.send_sems.at[self.used],
+            recv_sem=self.recv_sems.at[self.used],
+            device_id=device,
+            device_id_type=pl.DeviceIdType.MESH,
+        )
+        self.used += 1
+        copy.start()
+        self.copies.append(copy)
+        return copy
+
+    def finish(self):
+        for copy in self.copies:
+            copy.wait_send()
+
+
+def gather_index(place, done):
+    return tuple(
+        slice(None) if axis in done else place.at[axis] for axis in ("z", "y", "x", "c")
+    )
+
+
+def project_kernel(
+    kv_size, tp_size, x_ref, gain_ref, w0, w1, w2, w3, out_ref, sq_ref,
+    xg, scaled, part, yrecv, zpart, zrecv, sqpart, sqy, sqz, sqzrecv, send_sems, recv_sems,
+):
+    place = Place(kv_size, tp_size)
+    rows, block = x_ref.shape
+    greet(along(place, ("x", "c", "y", "z")))
+    sender = Sender(send_sems, recv_sems)
+    x, c, y, z = (place.at[axis] for axis in ("x", "c", "y", "z"))
+    sizes = place.sizes
+    copies = [
+        sender.start(x_ref, xg.at[x, c], place.device(x=place.partner("x", step)))
+        for step in range(1, sizes["x"])
+    ]
+    xg[x, c] = x_ref[...]
+    for copy in copies:
+        copy.wait_recv()
+    sender.start(xg.at[:, c], xg.at[:, c], place.device(c=place.partner("c", 1))).wait_recv()
+    squares = jnp.zeros((rows, block), F32)
+    for t in range(tp_size):
+        wide = xg[t // CORES, t % CORES].astype(F32)
+        squares += wide * wide
+        lanes = slice(t * block, (t + 1) * block)
+        scaled[:, lanes] = (wide * gain_ref[:, lanes]).astype(BF16)
+    sqpart[...] = squares.astype(BF16).reshape(sqpart.shape)
+
+    def y_stage(source, landing):
+        return [
+            sender.start(
+                source.at[:, place.partner("y", step)],
+                landing.at[step - 1],
+                place.device(y=place.partner("y", step)),
+            )
+            for step in range(1, sizes["y"])
+        ]
+
+    def y_sum(copies, source, landing):
+        for copy in copies:
+            copy.wait_recv()
+        total = source[:, y].astype(F32)
+        for step in range(1, sizes["y"]):
+            total += landing[step - 1].astype(F32)
+        return total.astype(BF16)
+
+    def z_stage(source, landing):
+        return [
+            sender.start(
+                source.at[place.partner("z", step)],
+                landing.at[step - 1],
+                place.device(z=place.partner("z", step)),
+            )
+            for step in range(1, sizes["z"])
+        ]
+
+    def z_sum(copies, source, landing):
+        for copy in copies:
+            copy.wait_recv()
+        total = source[z].astype(F32)
+        for step in range(1, sizes["z"]):
+            total += landing[step - 1].astype(F32)
+        return total
+
+    in_y = [y_stage(sqpart, sqy)]
+    for m, w in enumerate((w0, w1, w2, w3)):
+        product = jnp.dot(scaled[...], w[...], preferred_element_type=F32)
+        part[m] = product.astype(BF16).reshape(part.shape[1:])
+        in_y.append(y_stage(part.at[m], yrecv.at[m]))
+    sqz[...] = y_sum(in_y[0], sqpart, sqy)
+    in_z = [z_stage(sqz, sqzrecv)]
+    for m in range(4):
+        zpart[m] = y_sum(in_y[m + 1], part.at[m], yrecv.at[m])
+        in_z.append(z_stage(zpart.at[m], zrecv.at[m]))
+    sq_ref[...] = z_sum(in_z[0], sqz, sqzrecv)
+    for m in range(4):
+        out_ref[m] = z_sum(in_z[m + 1], zpart.at[m], zrecv.at[m])
+    sender.finish()
+
+
+def recur_kernel(
+    features, z_ref, sq_ref, state_ref, low_ref, shrink_ref, live_ref, lane_ref,
+    normed_ref, new_ref,
+):
+    sequences, heads, head, _ = state_ref.shape
+    rows = sequences * FRESH_PLACES
+    scale = lax.rsqrt(jnp.sum(sq_ref[...], axis=1, keepdims=True) / features + epsilon)
+    live = live_ref[...] > 0.5
+    slot = lax.broadcasted_iota(jnp.int32, (rows, head), 0) % FRESH_PLACES
+    owner = lax.broadcasted_iota(jnp.int32, (rows, head), 0) // FRESH_PLACES
+
+    def back(value, step, fill):
+        if step == 0:
+            return value
+        return jnp.where(slot >= step, pltpu.roll(value, step, 0), fill)
+
+    def ahead(value, step, fill):
+        return jnp.where(slot < FRESH_PLACES - step, pltpu.roll(value, rows - step, 0), fill)
+
+    for h in range(heads):
+        lanes = slice(h * head, (h + 1) * head)
+        zq, zf, v, zg = (z_ref[m, :, lanes] * scale for m in range(4))
+        query = zq * jax.nn.sigmoid(zq)
+        low = low_ref[:, lanes]
+        forget = low + (1.0 - low) * jax.nn.sigmoid(zf)
+        decay = jnp.where(live, jnp.exp(jnp.log(forget) + shrink_ref[:, lanes]), 1.0)
+        key = jnp.where(live, 1.0 - forget, 0.0)
+        prefix, suffix = decay, ahead(decay, 1, 1.0)
+        for step in (1, 2, 4):
+            prefix = prefix * back(prefix, step, 1.0)
+            suffix = suffix * ahead(suffix, step, 1.0)
+        out = jnp.sum(query * key, axis=1, keepdims=True) * v
+        weight = query
+        for step in range(1, FRESH_PLACES):
+            weight = weight * back(decay, step - 1, 0.0)
+            near = jnp.sum(weight * back(key, step, 0.0), axis=1, keepdims=True)
+            out += near * back(v, step, 0.0)
+        reach = (query * prefix).astype(BF16)
+        key_t = (key * suffix).T.astype(BF16)
+        prefix_t = prefix.T
+        v16 = v.astype(BF16)
+        old = []
+        for s in range(sequences):
+            mine = slice(s * FRESH_PLACES, (s + 1) * FRESH_PLACES)
+            before = state_ref[s, h]
+            old.append(
+                jnp.dot(reach[mine], before.astype(BF16), preferred_element_type=F32)
+            )
+            last = (s + 1) * FRESH_PLACES - 1
+            added = jnp.dot(
+                key_t, jnp.where(owner == s, v, 0.0).astype(BF16), preferred_element_type=F32
+            )
+            new_ref[s, h] = prefix_t[:, last : last + 1] * before + added
+        out += jnp.concatenate(old, axis=0)
+        out = out * lax.rsqrt(jnp.mean(out * out, axis=1, keepdims=True) + epsilon)
+        out = out * lane_ref[...] * (zg * jax.nn.sigmoid(zg))
+        normed_ref[:, lanes] = jnp.where(live, out, 0.0).astype(BF16)
+
+
+def attend_kernel(
+    kv_size, tp_size, n_ref, pick_ref, w_ref, x_ref, resid_ref,
+    ng, heads_part, landed, send_sems, recv_sems,
+):
+    place = Place(kv_size, tp_size)
+    sizes = place.sizes
+    z, y, x, c = (place.at[axis] for axis in ("z", "y", "x", "c"))
+    steps = [(i, j) for i in range(sizes["x"]) for j in range(CORES) if i or j]
+    across = [
+        (place.partner("x", i), place.partner("c", j)) for i, j in steps
+    ]
+    greet(along(place, ("z", "y")) + [place.device(x=i, c=j) for i, j in across])
+    sender = Sender(send_sems, recv_sems)
+    copies = [
+        sender.start(n_ref, ng.at[z, y], place.device(z=place.partner("z", step)))
+        for step in range(1, sizes["z"])
+    ]
+    ng[z, y] = n_ref[...]
+    for copy in copies:
+        copy.wait_recv()
+    copies = [
+        sender.start(ng.at[:, y], ng.at[:, y], place.device(y=place.partner("y", step)))
+        for step in range(1, sizes["y"])
+    ]
+    pick = pick_ref[...]
+    own = jnp.dot(pick, x_ref[...], preferred_element_type=F32)
+    for copy in copies:
+        copy.wait_recv()
+    every = ng[...].reshape(pick.shape[1], n_ref.shape[1])
+    chosen = jnp.dot(pick, every, preferred_element_type=F32).astype(BF16)
+    product = jnp.dot(chosen, w_ref[...], preferred_element_type=F32).astype(BF16)
+    block = x_ref.shape[1]
+    for t in range(tp_size):
+        heads_part[t] = product[:, t * block : (t + 1) * block]
+    copies = [
+        sender.start(heads_part.at[i * CORES + j], landed.at[n], place.device(x=i, c=j))
+        for n, (i, j) in enumerate(across)
+    ]
+    total = heads_part[x * CORES + c].astype(F32)
+    for n, copy in enumerate(copies):
+        copy.wait_recv()
+        total += landed[n].astype(F32)
+    resid_ref[...] = (own + total).astype(BF16)
+    sender.finish()
+
+
+def mixer_kernel(
+    kv_size, tp_size, x_ref, gain_ref, wg_hbm, wu_hbm, wd_hbm, out_ref,
+    xg, gg, wg, wu, wd, own_part, core_part, core_recv, recvs, parts,
+    send_sems, recv_sems, load_sems,
+):
+    place = Place(kv_size, tp_size)
+    sizes = place.sizes
+    at = place.at
+    rows, block = x_ref.shape
+    half = rows // 2
+    features = kv_size * tp_size * block
+    loads = [
+        pltpu.make_async_copy(source, target, load_sems.at[n])
+        for n, (source, target) in enumerate(((wg_hbm, wg), (wu_hbm, wu), (wd_hbm, wd)))
+    ]
+    for load in loads:
+        load.start()
+    greet(along(place, ("z", "y", "x", "c")))
+    sender = Sender(send_sems, recv_sems)
+
+    orders = (("z", "y", "x", "c"), ("z", "x", "y", "c"))
+
+    def view(ref, done, span):
+        lead = tuple(slice(None) if axis in done else at[axis] for axis in ("z", "y", "x"))
+        if "c" in done:
+            return ref.at[lead + (span, slice(None))]
+        return ref.at[lead + (span, pl.ds(pl.multiple_of(at["c"] * block, block), block))]
+
+    spans = [pl.ds(0, half), pl.ds(half, half)]
+
+    def push(h, level):
+        axis, done = orders[h][level], orders[h][:level]
+        started = []
+        for step in range(1, sizes[axis]):
+            device = place.device(**{axis: place.partner(axis, step)})
+            target = view(xg, done, spans[h])
+            source = x_ref.at[spans[h]] if level == 0 else target
+            started.append(sender.start(source, target, device))
+            if h == 0:
+                target = view(gg, done, slice(None))
+                started.append(sender.start(gain_ref if level == 0 else target, target, device))
+        return started
+
+    flying = [push(0, 0), push(1, 0)]
+    mine = pl.ds(pl.multiple_of(at["c"] * block, block), block)
+    xg[at["z"], at["y"], at["x"], :, mine] = x_ref[...]
+    gg[at["z"], at["y"], at["x"], :, mine] = gain_ref[...]
+    for level in range(1, 5):
+        for h in range(2):
+            for copy in flying[h]:
+                copy.wait_recv()
+            if level < 4:
+                flying[h] = push(h, level)
+    for load in loads:
+        load.wait()
+
+    units = [
+        (i, j, k)
+        for i in range(sizes["z"])
+        for j in range(sizes["y"])
+        for k in range(sizes["x"])
+    ]
+    wide = CORES * block
+    hidden_units = wg.shape[1]
+    gated = jnp.zeros((rows, hidden_units), F32)
+    upward = jnp.zeros((rows, hidden_units), F32)
+    squares = jnp.zeros((rows, wide), F32)
+    for n, unit in enumerate(units):
+        value = xg[unit].astype(F32)
+        squares += value * value
+        piece = (value * gg[unit][:1]).astype(BF16)
+        gated += jnp.dot(piece, wg[n * wide : (n + 1) * wide], preferred_element_type=F32)
+        upward += jnp.dot(piece, wu[n * wide : (n + 1) * wide], preferred_element_type=F32)
+    scale = lax.rsqrt(jnp.sum(squares, axis=1, keepdims=True) / features + epsilon)
+    gated, upward = gated * scale, upward * scale
+    hidden = (gated * jax.nn.sigmoid(gated) * upward).astype(BF16)
+
+    copies = []
+    for n, unit in enumerate(units):
+        product = jnp.dot(hidden, wd[:, n * wide : (n + 1) * wide], preferred_element_type=F32)
+        low, high = product[:, :block], product[:, block:]
+        first = at["c"] == 0
+        own_part[unit] = jnp.where(first, low, high)
+        core_part[unit] = jnp.where(first, high, low).astype(BF16)
+        if unit[1:] == (sizes["y"] - 1, sizes["x"] - 1):
+            copies.append(
+                sender.start(
+                    core_part.at[unit[0]], core_recv.at[unit[0]],
+                    place.device(c=place.partner("c", 1)),
+                )
+            )
+    for copy in copies:
+        copy.wait_recv()
+    sums = (("x", "y", "z"), ("y", "x", "z"))
+    axes = ("z", "y", "x")
+
+    def index(h, done, moved=None):
+        picked = []
+        for axis in axes:
+            if moved is not None and axis == moved[0]:
+                picked.append(moved[1])
+            elif axis in done:
+                picked.append(at[axis])
+            else:
+                picked.append(slice(None))
+        return tuple(picked)
+
+    def add_core(h):
+        span = slice(h * half, (h + 1) * half)
+        return own_part[:, :, :, span] + core_recv[:, :, :, span].astype(F32)
+
+    def send(h, level):
+        axis, done = sums[h][level], sums[h][:level]
+        source = parts[h][level]
+        keep = [a for a in axes if a not in done]
+        started = []
+        for step in range(1, sizes[axis]):
+            other = place.partner(axis, step)
+            where = tuple(other if a == axis else slice(None) for a in keep)
+            started.append(
+                sender.start(
+                    source.at[where] if where else source,
+                    recvs[h][level].at[step - 1],
+                    place.device(**{axis: other}),
+                )
+            )
+        return started
+
+    def reduce(h, level, copies):
+        axis, done = sums[h][level], sums[h][:level]
+        keep = [a for a in axes if a not in done]
+        where = tuple(at[a] if a == axis else slice(None) for a in keep)
+        for copy in copies:
+            copy.wait_recv()
+        total = parts[h][level][where].astype(F32)
+        for step in range(1, sizes[axis]):
+            total += recvs[h][level][step - 1].astype(F32)
+        return total
+
+    flying = []
+    for h in range(2):
+        parts[h][0][...] = add_core(h).astype(BF16)
+        flying.append(send(h, 0))
+    for level in range(2):
+        for h in range(2):
+            parts[h][level + 1][...] = reduce(h, level, flying[h]).astype(BF16)
+            flying[h] = send(h, level + 1)
+    for h in range(2):
+        span = slice(h * half, (h + 1) * half)
+        down = reduce(h, 2, flying[h])
+        out_ref[span] = (x_ref[span].astype(F32) + down).astype(BF16)
+    sender.finish()
+
+
+def remote(kernel, out_shape, specs, scratch, name, identity):
+    return pl.pallas_call(
+        kernel,
+        out_shape=out_shape,
+        in_specs=specs,
+        out_specs=jax.tree.map(lambda _: VM, out_shape),
+        scratch_shapes=scratch,
+        compiler_params=pltpu.CompilerParams(
+            collective_id=identity, has_side_effects=True, vmem_limit_bytes=LIMIT
+        ),
+        name=name,
+    )
+
 
 def local(
+    kv_size,
+    tp_size,
+    residual_entries,
+    fresh_extents,
+    memory_matrix,
+    initial_rescale_vector,
+    probe_matrix,
+    retain_matrix,
+    content_matrix,
+    result_switch_matrix,
+    retain_lower_limit,
+    extra_shrink_log,
+    lane_result_rescale,
+    result_matrix,
+    later_rescale_vector,
+    mixer_switch_matrix,
+    widening_matrix,
+    narrowing_matrix,
+):
+    sequences, heads, head, _ = memory_matrix.shape
+    own_rows = sequences * FRESH_PLACES
+    all_rows, block = residual_entries.shape
+    live_count = all_rows // 2
+    width = probe_matrix.shape[1]
+    features = block * kv_size * tp_size
+    kv_index = lax.axis_index("kv")
+    nz = 4 if kv_size % 4 == 0 else kv_size
+    ny, nx = kv_size // nz, tp_size // CORES
+    dma = pltpu.SemaphoreType.DMA
+
+    strings = fresh_extents.shape[0]
+    earlier = jnp.arange(strings)[:, None] < jnp.arange(strings)[None, :]
+    starts = jnp.sum(jnp.where(earlier, fresh_extents[:, None], 0), axis=0)
+    places = jnp.arange(FRESH_PLACES, dtype=jnp.int32)[None, :]
+    living = places < fresh_extents[:, None]
+    rank = jnp.where(living, starts[:, None] + places, -1).reshape(1, all_rows)
+    pick = (rank == jnp.arange(live_count, dtype=jnp.int32)[:, None]).astype(BF16)
+
+    count = (nx - 1) + 1 + 5 * (ny - 1 + nz - 1)
+    projected, squares = remote(
+        functools.partial(project_kernel, kv_size, tp_size),
+        (
+            jax.ShapeDtypeStruct((4, own_rows, width), F32),
+            jax.ShapeDtypeStruct((own_rows, block), F32),
+        ),
+        [VM] * 6,
+        [
+            pltpu.VMEM((nx, CORES, all_rows, block), BF16),
+            pltpu.VMEM((all_rows, tp_size * block), BF16),
+            pltpu.VMEM((4, nz, ny, own_rows, width), BF16),
+            pltpu.VMEM((4, max(ny - 1, 1), nz, own_rows, width), BF16),
+            pltpu.VMEM((4, nz, own_rows, width), BF16),
+            pltpu.VMEM((4, max(nz - 1, 1), own_rows, width), BF16),
+            pltpu.VMEM((nz, ny, own_rows, block), BF16),
+            pltpu.VMEM((max(ny - 1, 1), nz, own_rows, block), BF16),
+            pltpu.VMEM((nz, own_rows, block), BF16),
+            pltpu.VMEM((max(nz - 1, 1), own_rows, block), BF16),
+            dma((count,)),
+            dma((count,)),
+        ],
+        "project",
+        1,
+    )(
+        residual_entries,
+        initial_rescale_vector.reshape(1, -1),
+        probe_matrix,
+        retain_matrix,
+        content_matrix,
+        result_switch_matrix,
+    )
+
+    own_living = lax.dynamic_slice_in_dim(living, kv_index * sequences, sequences)
+    live = jnp.broadcast_to(own_living.reshape(own_rows, 1), (own_rows, head)).astype(F32)
+    shrink = jnp.repeat(extra_shrink_log, head, axis=1)
+    normed, new_state = pl.pallas_call(
+        functools.partial(recur_kernel, features),
+        out_shape=(
+            jax.ShapeDtypeStruct((own_rows, width), BF16),
+            jax.ShapeDtypeStruct(memory_matrix.shape, F32),
+        ),
+        in_specs=[VM] * 7,
+        out_specs=(VM, VM),
+        compiler_params=pltpu.CompilerParams(vmem_limit_bytes=LIMIT),
+        name="recur",
+    )(
+        projected,
+        squares,
+        memory_matrix,
+        retain_lower_limit.reshape(1, -1),
+        shrink,
+        live,
+        lane_result_rescale.reshape(1, -1),
+    )
+
+    count = (nz - 1) + (ny - 1) + (tp_size - 1)
+    residual = remote(
+        functools.partial(attend_kernel, kv_size, tp_size),
+        jax.ShapeDtypeStruct((live_count, block), BF16),
+        [VM] * 4,
+        [
+            pltpu.VMEM((nz, ny, own_rows, width), BF16),
+            pltpu.VMEM((tp_size, live_count, block), BF16),
+            pltpu.VMEM((tp_size - 1, live_count, block), BF16),
+            dma((count,)),
+            dma((count,)),
+        ],
+        "attend",
+        2,
+    )(normed, pick, result_matrix, residual_entries)
+
+    half = live_count // 2
+    sizes = {"z": nz, "y": ny, "x": nx}
+
+    def buffers(order):
+        left, landing, kept = ["z", "y", "x"], [], []
+        for axis in order:
+            kept.append(pltpu.VMEM(tuple(sizes[a] for a in left) + (half, block), BF16))
+            left = [a for a in left if a != axis]
+            landing.append(
+                pltpu.VMEM(
+                    (max(sizes[axis] - 1, 1),) + tuple(sizes[a] for a in left) + (half, block),
+                    BF16,
+                )
+            )
+        return kept, landing
+
+    first, second = buffers(("x", "y", "z")), buffers(("y", "x", "z"))
+    hops = nz + ny + nx - 3
+    count = 3 * (hops + 1) + nz + 2 * hops
+    hidden_units = mixer_switch_matrix.shape[1]
+    mixed_live = remote(
+        functools.partial(mixer_kernel, kv_size, tp_size),
+        jax.ShapeDtypeStruct((live_count, block), BF16),
+        [VM, VM, HBM, HBM, HBM],
+        [
+            pltpu.VMEM((nz, ny, nx, live_count, CORES * block), BF16),
+            pltpu.VMEM((nz, ny, nx, 8, CORES * block), F32),
+            pltpu.VMEM((features, hidden_units), BF16),
+            pltpu.VMEM((features, hidden_units), BF16),
+            pltpu.VMEM((hidden_units, features), BF16),
+            pltpu.VMEM((nz, ny, nx, live_count, block), F32),
+            pltpu.VMEM((nz, ny, nx, live_count, block), BF16),
+            pltpu.VMEM((nz, ny, nx, live_count, block), BF16),
+            [first[1], second[1]],
+            [first[0], second[0]],
+            dma((count,)),
+            dma((count,)),
+            dma((3,)),
+        ],
+        "mixer",
+        3,
+    )(
+        residual,
+        jnp.broadcast_to(later_rescale_vector.reshape(1, -1), (8, block)),
+        mixer_switch_matrix,
+        widening_matrix,
+        narrowing_matrix,
+    )
+    mixed = jnp.dot(pick.T, mixed_live, preferred_element_type=F32).astype(BF16)
+    return (mixed, new_state)
+
+
+def plain_local(
     residual_entries,
     fresh_extents,
     memory_matrix,
@@ -33,12 +619,13 @@
     heads_per_device = memory_matrix.shape[1]
     rows_dev = sequences_per_device * FRESH_PLACES
     all_rows = residual_entries.shape[0]
+    features = initial_rescale_vector.shape[0] * lax.axis_size("kv")
     kv_index = lax.axis_index("kv")
     tokens_wide = residual_entries.astype(jnp.float32)
     columns = lax.all_gather(residual_entries, "tp", axis=1, tiled=True)
     squares = lax.psum(jnp.sum(tokens_wide * tokens_wide, axis=1), ("kv", "tp"))
     own_squares = lax.dynamic_slice_in_dim(squares, kv_index * rows_dev, rows_dev)
-    first_scale = lax.rsqrt(own_squares / D + epsilon)
+    first_scale = lax.rsqrt(own_squares / features + epsilon)
     scaled = (columns.astype(jnp.float32) * initial_rescale_vector).astype(jnp.bfloat16)
     projected = (
         lax.psum_scatter(
@@ -61,7 +648,7 @@
         * first_scale[:, None]
     )
     width_dev = probe_matrix.shape[1]
-    shape_four = (sequences_per_device, FRESH_PLACES, heads_per_device, HEAD)
+    shape_four = (sequences_per_device, FRESH_PLACES, heads_per_device, memory_matrix.shape[2])
     z_query = projected[:, :width_dev]
     z_forget = projected[:, width_dev : 2 * width_dev].reshape(shape_four)
     z_input = projected[:, 2 * width_dev : 3 * width_dev].reshape(shape_four)
@@ -71,7 +658,7 @@
     )
     living = jnp.arange(FRESH_PLACES, dtype=jnp.int32)[None, :] < own_lengths[:, None]
     query = jax.nn.silu(z_query).reshape(shape_four)
-    bounds = retain_lower_limit.reshape(heads_per_device, HEAD)
+    bounds = retain_lower_limit.reshape(heads_per_device, memory_matrix.shape[2])
     retain_factor = bounds + (1.0 - bounds) * jax.nn.sigmoid(z_forget)
     shrink_exponent = jnp.log(retain_factor) + extra_shrink_log.reshape(
         sequences_per_device, FRESH_PLACES, heads_per_device, 1
@@ -113,7 +700,7 @@
     resid_wide = residual.astype(jnp.float32)
     resid_squares = lax.psum(jnp.sum(resid_wide * resid_wide, axis=1), ("kv", "tp"))
     second_in = (
-        resid_wide * later_rescale_vector * lax.rsqrt(resid_squares / D + epsilon)[:, None]
+        resid_wide * later_rescale_vector * lax.rsqrt(resid_squares / features + epsilon)[:, None]
     ).astype(jnp.bfloat16)
     live_rows = (
         jnp.arange(FRESH_PLACES, dtype=jnp.int32)[None, :] < fresh_extents[:, None]
@@ -156,8 +743,15 @@
         P(None, ("kv", "tp")),
         P(("kv", "tp"), None),
     )
+
+    def step(residual_entries, *others):
+        sizes = mesh.shape["kv"], mesh.shape["tp"]
+        if residual_entries.shape[1] % 128:
+            return plain_local(residual_entries, *others)
+        return local(*sizes, residual_entries, *others)
+
     return jax.shard_map(
-        local,
+        step,
         mesh=mesh,
         in_specs=placed,
         out_specs=(P(None, ("kv", "tp")), P("kv", "tp", None, None)),

time: 449 us -> 136 us (0.30)
  waiting for transfers between devices: 241 us -> 0 us
  blocking collectives: 120 us -> 0 us
  Pallas kernels: 0 us -> 119 us
  matrix products: 45.2 us -> 1.85 us
  other arithmetic: 18.2 us -> 2.97 us
  between operations: 14.2 us -> 0.7 us
    reduce_scatter x2 -> x0, waiting for transfers between devices: 171 us -> none  [the longest x1 142 us: local(): lax.psum_scatter(jnp.dot(hidden, narrowing_matrix, preferred_element_type...]
    pallas_call x0 -> x4, Pallas kernels: none -> 119 us  [the longest x1 47.5 us: local(): remote(functools.partial(mixer_kernel, kv_size, tp_size), jax.ShapeDtypeS...]
    psum x2 -> x0, blocking collectives: 80.1 us -> none  [the longest x1 40.8 us: local(): squares = lax.psum(jnp.sum(tokens_wide * tokens_wide, axis=1), ('kv', 'tp'))]
    all_gather x1 -> x0, waiting for transfers between devices: 53.8 us -> none  [local(): piece = lax.all_gather(mixer_input, ('kv', 'tp'), axis=1, tiled=True)]
    dot_general x15 -> x1, matrix products: 45.2 us -> 1.85 us  [local(): mixed = jnp.dot(pick.T, mixed_live, preferred_element_type=F32).astype(BF16)]
    all_gather x2 -> x0, blocking collectives: 40.3 us -> none  [the longest x1 31.3 us: local(): lax.all_gather(normed, 'kv', axis=0, tiled=True)]
    unnamed x5 -> x0, waiting for transfers between devices: 16.8 us -> none
    add x1 -> x0, other arithmetic: 8.99 us -> none  [local(): decays[:, position, :, :, None] * carried]
  transfers between devices with their start and end apart: 4 -> 0, of which waited for: 4 -> 0; matrix products, arithmetic and copies ran while one was open for 1% -> 0% of each run, Pallas kernels for 0% -> 0%
where the time goes in v1:
time: 136 us; the launch traced here: 135 us
  Pallas kernels  119 us (88%)
  local copies, waits for them, and re-layouts  11.1 us (8%)
  other arithmetic  2.97 us (2%)
  matrix products  1.85 us (1%)
    pallas_call x1, Pallas kernels, local(): remote(functools.partial(mixer_kernel, kv_size, tp_size), jax.ShapeDtypeS...  47.5 us
    pallas_call x1, Pallas kernels, local(): remote(functools.partial(project_kernel, kv_size, tp_size), (jax.ShapeDty...  45.1 us
    pallas_call x1, Pallas kernels, local(): remote(functools.partial(attend_kernel, kv_size, tp_size), jax.ShapeDtype...  21.2 us
    unnamed x6, local copies, waits for them, and re-layouts  8.86 us
    pallas_call x1, Pallas kernels, local(): pl.pallas_call(functools.partial(recur_kernel, features), out_shape=(jax....  4.92 us

profile of v1, /device:TPU:0, one launch (start us, length us, event | category | flops | bytes accessed | tf_op | source)
XLA Modules:
  0.0 135.4 jit_solution(9561702736377683544)
XLA Ops:
  0.6 0.7 select_reduce_fusion
  1.4 1.2 broadcast_in_dim.41.gain_ref
  2.6 0.7 iota_compare_fusion.3
  3.4 0.1 reshape.60
  3.5 0.7 broadcast_in_dim.40.live_ref
  4.2 0.7 add_select_fusion
  4.9 0.1 select_n.20
  5.0 0.8 copy.24
  5.8 0.1 broadcast_in_dim.39
  5.9 0.7 copy.29
  6.6 0.7 fusion.pick_ref
  7.3 0.0 copy-start
  7.3 45.1 %project.1 = (f32[4,64,512]{2,1,0:T(8,128)}, f32[64,128]{1,0:T(8,128)}) custom-call(bf16[512,128]{1,0:T(8,128)(2,1)} %x_ref.3, f32[1,512]{1,0:T(1,128)} %bitcast.10, bf16[512,512]{1,0:T(8,128)(2,1)} %w0.1, bf16[512,512]{1,0:T(8,128)(2,1)} %w1.1, bf16[512,512]{1,0:T(8,128)(2,1)} %w2.1, bf16[512,512]{1,0:T(8,128)(2,1)} %w3.1), custom_call_target="tpu_custom_call" | custom-call | tf_op jit(solution)/shard_map/project/pallas_call | solution.py:477
  52.4 4.9 %recur.1 = (bf16[64,512]{1,0:T(8,128)(2,1)}, f32[8,4,128,128]{3,2,1,0:T(8,128)}) custom-call(f32[4,64,512]{2,1,0:T(8,128)} %get-tuple-element.6.z_ref, f32[64,128]{1,0:T(8,128)} %get-tuple-element.7.sq_ref, f32[8,4,128,128]{3,2,1,0:T(8,128)} %state_ref.1, f32[1,512]{1,0:T(1,128)} %bitcast.11, f32[64,512]{1,0:T(8,128)} %bitcast.9, ...), custom_call_target="tpu_custom_call" | custom-call | tf_op jit(solution)/shard_map/recur/pallas_call | solution.py:512
  57.3 21.2 %attend.1.x_ref = bf16[256,128]{1,0:T(8,128)(2,1)} custom-call(bf16[64,512]{1,0:T(8,128)(2,1)} %get-tuple-element.8.n_ref, bf16[256,512]{1,0:T(8,128)(2,1)} %fusion.pick_ref, bf16[512,512]{1,0:T(8,128)(2,1)} %w_ref.1, bf16[512,128]{1,0:T(8,128)(2,1)} %x_ref.3), custom_call_target="tpu_custom_call" | custom-call | tf_op jit(solution)/shard_map/attend/pallas_call | solution.py:533
  78.6 0.0 copy-done
  78.6 2.8 %copy.25.wg_hbm = bf16[4096,344]{1,0:T(8,128)(2,1)} copy(bf16[4096,344]{0,1:T(8,128)(2,1)S(1)} %copy-done) | data formatting | bytes 5636096 | tf_op args[13]
  81.4 4.6 %copy.26.wu_hbm = bf16[4096,344]{1,0:T(8,128)(2,1)} copy(bf16[4096,344]{0,1:T(8,128)(2,1)} %param.30) | data formatting | bytes 5636096 | tf_op args[14]
  86.0 47.5 %mixer.1 = bf16[256,128]{1,0:T(8,128)(2,1)} custom-call(bf16[256,128]{1,0:T(8,128)(2,1)} %attend.1.x_ref, f32[8,128]{1,0:T(8,128)} %broadcast_in_dim.41.gain_ref, bf16[4096,344]{1,0:T(8,128)(2,1)} %copy.25.wg_hbm, bf16[4096,344]{1,0:T(8,128)(2,1)} %copy.26.wu_hbm, bf16[344,4096]{1,0:T(8,128)(2,1)} %wd_hbm.1), custom_call_target="tpu_custom_call" | custom-call | tf_op jit(solution)/shard_map/mixer/pallas_call | solution.py:568
  133.5 1.8 %convolution_convert_fusion = bf16[512,128]{1,0:T(8,128)(2,1)} fusion(bf16[256,128]{1,0:T(8,128)(2,1)} %mixer.1, s32[512]{0:T(512)S(1)} %select_n.20), kind=kOutput, calls=%fused_computation | convolution fusion | flops 33751040 | bytes 198656 | tf_op jit(solution)/shard_map/dot_general | solution.py:596
  (1 shorter events, 0.0 us)
Async XLA Ops:
  7.3 71.2 %copy-start = (bf16[4096,344]{0,1:T(8,128)(2,1)S(1)}, bf16[4096,344]{0,1:T(8,128)(2,1)}, u32[]{:S(2)}) copy-start(bf16[4096,344]{0,1:T(8,128)(2,1)} %param.29) | copy-start | bytes 8454148

commit v2 on v1

--- a/solution.py
+++ b/solution.py
@@ -9,6 +9,7 @@
 
 FRESH_PLACES = 8
 CORES = 2
+PIECES = 8
 epsilon = 1e-06
 
 F32, BF16 = jnp.float32, jnp.bfloat16
@@ -146,31 +147,43 @@
         return total
 
     in_y = [y_stage(sqpart, sqy)]
-    for m, w in enumerate((w0, w1, w2, w3)):
-        product = jnp.dot(scaled[...], w[...], preferred_element_type=F32)
+    chunk = part.shape[-1]
+    for m in range(PIECES):
+        w, lanes = (w0, w1, w2, w3)[m // 2], slice(m % 2 * chunk, (m % 2 + 1) * chunk)
+        product = jnp.dot(scaled[...], w[:, lanes], preferred_element_type=F32)
         part[m] = product.astype(BF16).reshape(part.shape[1:])
         in_y.append(y_stage(part.at[m], yrecv.at[m]))
     sqz[...] = y_sum(in_y[0], sqpart, sqy)
     in_z = [z_stage(sqz, sqzrecv)]
-    for m in range(4):
+    for m in range(PIECES):
         zpart[m] = y_sum(in_y[m + 1], part.at[m], yrecv.at[m])
         in_z.append(z_stage(zpart.at[m], zrecv.at[m]))
     sq_ref[...] = z_sum(in_z[0], sqz, sqzrecv)
-    for m in range(4):
-        out_ref[m] = z_sum(in_z[m + 1], zpart.at[m], zrecv.at[m])
+    for m in range(PIECES):
+        out_ref[m // 2, :, m % 2 * chunk : (m % 2 + 1) * chunk] = z_sum(in_z[m + 1], zpart.at[m], zrecv.at[m])
     sender.finish()
 
 
 def recur_kernel(
-    features, z_ref, sq_ref, state_ref, low_ref, shrink_ref, live_ref, lane_ref,
-    normed_ref, new_ref,
+    features, z_ref, sq_ref, state_ref, low_ref, shrink_ref, extent_ref, lane_ref, gain_ref,
+    normed_ref, new_ref, gain_rows_ref,
 ):
     sequences, heads, head, _ = state_ref.shape
     rows = sequences * FRESH_PLACES
     scale = lax.rsqrt(jnp.sum(sq_ref[...], axis=1, keepdims=True) / features + epsilon)
-    live = live_ref[...] > 0.5
+    gain_rows_ref[...] = jnp.broadcast_to(gain_ref[...], gain_rows_ref.shape)
+    strings = extent_ref.shape[1]
+    string = lax.broadcasted_iota(jnp.int32, (rows, strings), 1)
+    row = lax.broadcasted_iota(jnp.int32, (rows, strings), 0)
+    first = lax.axis_index("kv") * sequences
+    extent = jnp.sum(
+        jnp.where(string == first + row // FRESH_PLACES, extent_ref[...].astype(F32), 0.0),
+        axis=1, keepdims=True,
+    )
     slot = lax.broadcasted_iota(jnp.int32, (rows, head), 0) % FRESH_PLACES
     owner = lax.broadcasted_iota(jnp.int32, (rows, head), 0) // FRESH_PLACES
+
+    live = slot.astype(F32) < extent
 
     def back(value, step, fill):
         if step == 0:
@@ -186,7 +199,7 @@
         query = zq * jax.nn.sigmoid(zq)
         low = low_ref[:, lanes]
         forget = low + (1.0 - low) * jax.nn.sigmoid(zf)
-        decay = jnp.where(live, jnp.exp(jnp.log(forget) + shrink_ref[:, lanes]), 1.0)
+        decay = jnp.where(live, jnp.exp(jnp.log(forget) + shrink_ref[:, h : h + 1]), 1.0)
         key = jnp.where(live, 1.0 - forget, 0.0)
         prefix, suffix = decay, ahead(decay, 1, 1.0)
         for step in (1, 2, 4):
@@ -220,8 +233,39 @@
         normed_ref[:, lanes] = jnp.where(live, out, 0.0).astype(BF16)
 
 
+def pick_rows(extent_ref, count, total):
+    strings = extent_ref.shape[1]
+    extents = jnp.broadcast_to(extent_ref[...].astype(F32), (16, strings)).astype(BF16)
+    string = lax.broadcasted_iota(jnp.int32, (strings, total), 0)
+    owner = lax.broadcasted_iota(jnp.int32, (strings, total), 1) // FRESH_PLACES
+    one, none = jnp.ones((), F32), jnp.zeros((), F32)
+    start = jnp.dot(
+        extents, jnp.where(string < owner, one, none).astype(BF16), preferred_element_type=F32
+    )[:1]
+    extent = jnp.dot(
+        extents, jnp.where(string == owner, one, none).astype(BF16), preferred_element_type=F32
+    )[:1]
+    slot = (lax.broadcasted_iota(jnp.int32, (1, total), 1) % FRESH_PLACES).astype(F32)
+    rank = jnp.where(slot < extent, start + slot, -1.0)
+    row = lax.broadcasted_iota(jnp.int32, (count, total), 0).astype(F32)
+    return jnp.where(rank == row, one, none).astype(BF16)
+
+
+def place_rows(extent_ref, count, total):
+    strings = extent_ref.shape[1]
+    extents = extent_ref[...].astype(F32)
+    string = lax.broadcasted_iota(jnp.int32, (total, strings), 1)
+    owner = lax.broadcasted_iota(jnp.int32, (total, strings), 0) // FRESH_PLACES
+    start = jnp.sum(jnp.where(string < owner, extents, 0.0), axis=1, keepdims=True)
+    extent = jnp.sum(jnp.where(string == owner, extents, 0.0), axis=1, keepdims=True)
+    slot = (lax.broadcasted_iota(jnp.int32, (total, 1), 0) % FRESH_PLACES).astype(F32)
+    rank = jnp.where(slot < extent, start + slot, -1.0)
+    row = lax.broadcasted_iota(jnp.int32, (total, count), 1).astype(F32)
+    return jnp.where(rank == row, 1.0, 0.0).astype(BF16)
+
+
 def attend_kernel(
-    kv_size, tp_size, n_ref, pick_ref, w_ref, x_ref, resid_ref,
+    kv_size, tp_size, n_ref, extent_ref, w_ref, x_ref, resid_ref,
     ng, heads_part, landed, send_sems, recv_sems,
 ):
     place = Place(kv_size, tp_size)
@@ -233,20 +277,31 @@
     ]
     greet(along(place, ("z", "y")) + [place.device(x=i, c=j) for i, j in across])
     sender = Sender(send_sems, recv_sems)
-    copies = [
-        sender.start(n_ref, ng.at[z, y], place.device(z=place.partner("z", step)))
-        for step in range(1, sizes["z"])
+    half = n_ref.shape[0] // 2
+    spans = [pl.ds(0, half), pl.ds(half, half)]
+    in_z = [
+        [
+            sender.start(
+                n_ref.at[span], ng.at[z, y, span], place.device(z=place.partner("z", step))
+            )
+            for step in range(1, sizes["z"])
+        ]
+        for span in spans
     ]
     ng[z, y] = n_ref[...]
-    for copy in copies:
-        copy.wait_recv()
-    copies = [
-        sender.start(ng.at[:, y], ng.at[:, y], place.device(y=place.partner("y", step)))
-        for step in range(1, sizes["y"])
-    ]
-    pick = pick_ref[...]
+    pick = pick_rows(extent_ref, resid_ref.shape[0], x_ref.shape[0])
     own = jnp.dot(pick, x_ref[...], preferred_element_type=F32)
-    for copy in copies:
+    in_y = []
+    for span, copies in zip(spans, in_z):
+        for copy in copies:
+            copy.wait_recv()
+        in_y += [
+            sender.start(
+                ng.at[:, y, span], ng.at[:, y, span], place.device(y=place.partner("y", step))
+            )
+            for step in range(1, sizes["y"])
+        ]
+    for copy in in_y:
         copy.wait_recv()
     every = ng[...].reshape(pick.shape[1], n_ref.shape[1])
     chosen = jnp.dot(pick, every, preferred_element_type=F32).astype(BF16)
@@ -267,7 +322,7 @@
 
 
 def mixer_kernel(
-    kv_size, tp_size, x_ref, gain_ref, wg_hbm, wu_hbm, wd_hbm, out_ref,
+    kv_size, tp_size, x_ref, gain_ref, extent_ref, wg_hbm, wu_hbm, wd_hbm, out_ref,
     xg, gg, wg, wu, wd, own_part, core_part, core_recv, recvs, parts,
     send_sems, recv_sems, load_sems,
 ):
@@ -313,6 +368,7 @@
     mine = pl.ds(pl.multiple_of(at["c"] * block, block), block)
     xg[at["z"], at["y"], at["x"], :, mine] = x_ref[...]
     gg[at["z"], at["y"], at["x"], :, mine] = gain_ref[...]
+    spread = place_rows(extent_ref, rows, out_ref.shape[0])
     for level in range(1, 5):
         for h in range(2):
             for copy in flying[h]:
@@ -329,16 +385,22 @@
         for k in range(sizes["x"])
     ]
     wide = CORES * block
-    hidden_units = wg.shape[1]
+    hidden_units = wg.shape[0]
     gated = jnp.zeros((rows, hidden_units), F32)
     upward = jnp.zeros((rows, hidden_units), F32)
     squares = jnp.zeros((rows, wide), F32)
+
+    def across(left, right):
+        return lax.dot_general(
+            left, right, (((1,), (1,)), ((), ())), preferred_element_type=F32
+        )
+
     for n, unit in enumerate(units):
         value = xg[unit].astype(F32)
         squares += value * value
         piece = (value * gg[unit][:1]).astype(BF16)
-        gated += jnp.dot(piece, wg[n * wide : (n + 1) * wide], preferred_element_type=F32)
-        upward += jnp.dot(piece, wu[n * wide : (n + 1) * wide], preferred_element_type=F32)
+        gated += across(piece, wg[:, n * wide : (n + 1) * wide])
+        upward += across(piece, wu[:, n * wide : (n + 1) * wide])
     scale = lax.rsqrt(jnp.sum(squares, axis=1, keepdims=True) / features + epsilon)
     gated, upward = gated * scale, upward * scale
     hidden = (gated * jax.nn.sigmoid(gated) * upward).astype(BF16)
@@ -413,10 +475,9 @@
         for h in range(2):
             parts[h][level + 1][...] = reduce(h, level, flying[h]).astype(BF16)
             flying[h] = send(h, level + 1)
-    for h in range(2):
-        span = slice(h * half, (h + 1) * half)
-        down = reduce(h, 2, flying[h])
-        out_ref[span] = (x_ref[span].astype(F32) + down).astype(BF16)
+    down = jnp.concatenate([reduce(h, 2, flying[h]) for h in range(2)], axis=0)
+    mixed = (x_ref[...].astype(F32) + down).astype(BF16)
+    out_ref[...] = jnp.dot(spread, mixed, preferred_element_type=F32).astype(BF16)
     sender.finish()
 
 
@@ -460,20 +521,12 @@
     live_count = all_rows // 2
     width = probe_matrix.shape[1]
     features = block * kv_size * tp_size
-    kv_index = lax.axis_index("kv")
     nz = 4 if kv_size % 4 == 0 else kv_size
     ny, nx = kv_size // nz, tp_size // CORES
     dma = pltpu.SemaphoreType.DMA
 
-    strings = fresh_extents.shape[0]
-    earlier = jnp.arange(strings)[:, None] < jnp.arange(strings)[None, :]
-    starts = jnp.sum(jnp.where(earlier, fresh_extents[:, None], 0), axis=0)
-    places = jnp.arange(FRESH_PLACES, dtype=jnp.int32)[None, :]
-    living = places < fresh_extents[:, None]
-    rank = jnp.where(living, starts[:, None] + places, -1).reshape(1, all_rows)
-    pick = (rank == jnp.arange(live_count, dtype=jnp.int32)[:, None]).astype(BF16)
-
-    count = (nx - 1) + 1 + 5 * (ny - 1 + nz - 1)
+    piece = 4 * width // PIECES
+    count = (nx - 1) + 1 + (PIECES + 1) * (ny - 1 + nz - 1)
     projected, squares = remote(
         functools.partial(project_kernel, kv_size, tp_size),
         (
@@ -484,10 +537,10 @@
         [
             pltpu.VMEM((nx, CORES, all_rows, block), BF16),
             pltpu.VMEM((all_rows, tp_size * block), BF16),
-            pltpu.VMEM((4, nz, ny, own_rows, width), BF16),
-            pltpu.VMEM((4, max(ny - 1, 1), nz, own_rows, width), BF16),
-            pltpu.VMEM((4, nz, own_rows, width), BF16),
-            pltpu.VMEM((4, max(nz - 1, 1), own_rows, width), BF16),
+            pltpu.VMEM((PIECES, nz, ny, own_rows, piece), BF16),
+            pltpu.VMEM((PIECES, max(ny - 1, 1), nz, own_rows, piece), BF16),
+            pltpu.VMEM((PIECES, nz, own_rows, piece), BF16),
+            pltpu.VMEM((PIECES, max(nz - 1, 1), own_rows, piece), BF16),
             pltpu.VMEM((nz, ny, own_rows, block), BF16),
             pltpu.VMEM((max(ny - 1, 1), nz, own_rows, block), BF16),
             pltpu.VMEM((nz, own_rows, block), BF16),
@@ -506,17 +559,16 @@
         result_switch_matrix,
     )
 
-    own_living = lax.dynamic_slice_in_dim(living, kv_index * sequences, sequences)
-    live = jnp.broadcast_to(own_living.reshape(own_rows, 1), (own_rows, head)).astype(F32)
-    shrink = jnp.repeat(extra_shrink_log, head, axis=1)
-    normed, new_state = pl.pallas_call(
+    extents = fresh_extents.reshape(1, -1)
+    normed, new_state, gain_rows = pl.pallas_call(
         functools.partial(recur_kernel, features),
         out_shape=(
             jax.ShapeDtypeStruct((own_rows, width), BF16),
             jax.ShapeDtypeStruct(memory_matrix.shape, F32),
+            jax.ShapeDtypeStruct((8, block), F32),
         ),
-        in_specs=[VM] * 7,
-        out_specs=(VM, VM),
+        in_specs=[VM] * 8,
+        out_specs=(VM, VM, VM),
         compiler_params=pltpu.CompilerParams(vmem_limit_bytes=LIMIT),
         name="recur",
     )(
@@ -524,12 +576,13 @@
         squares,
         memory_matrix,
         retain_lower_limit.reshape(1, -1),
-        shrink,
-        live,
+        extra_shrink_log,
+        extents,
         lane_result_rescale.reshape(1, -1),
-    )
-
-    count = (nz - 1) + (ny - 1) + (tp_size - 1)
+        later_rescale_vector.reshape(1, -1),
+    )
+
+    count = 2 * (nz - 1) + 2 * (ny - 1) + (tp_size - 1)
     residual = remote(
         functools.partial(attend_kernel, kv_size, tp_size),
         jax.ShapeDtypeStruct((live_count, block), BF16),
@@ -543,7 +596,7 @@
         ],
         "attend",
         2,
-    )(normed, pick, result_matrix, residual_entries)
+    )(normed, extents, result_matrix, residual_entries)
 
     half = live_count // 2
     sizes = {"z": nz, "y": ny, "x": nx}
@@ -565,15 +618,15 @@
     hops = nz + ny + nx - 3
     count = 3 * (hops + 1) + nz + 2 * hops
     hidden_units = mixer_switch_matrix.shape[1]
-    mixed_live = remote(
+    mixed = remote(
         functools.partial(mixer_kernel, kv_size, tp_size),
-        jax.ShapeDtypeStruct((live_count, block), BF16),
-        [VM, VM, HBM, HBM, HBM],
+        jax.ShapeDtypeStruct((all_rows, block), BF16),
+        [VM, VM, VM, HBM, HBM, HBM],
         [
             pltpu.VMEM((nz, ny, nx, live_count, CORES * block), BF16),
             pltpu.VMEM((nz, ny, nx, 8, CORES * block), F32),
-            pltpu.VMEM((features, hidden_units), BF16),
-            pltpu.VMEM((features, hidden_units), BF16),
+            pltpu.VMEM((hidden_units, features), BF16),
+            pltpu.VMEM((hidden_units, features), BF16),
             pltpu.VMEM((hidden_units, features), BF16),
             pltpu.VMEM((nz, ny, nx, live_count, block), F32),
             pltpu.VMEM((nz, ny, nx, live_count, block), BF16),
@@ -588,12 +641,12 @@
         3,
     )(
         residual,
-        jnp.broadcast_to(later_rescale_vector.reshape(1, -1), (8, block)),
-        mixer_switch_matrix,
-        widening_matrix,
+        gain_rows,
+        extents,
+        mixer_switch_matrix.T,
+        widening_matrix.T,
         narrowing_matrix,
     )
-    mixed = jnp.dot(pick.T, mixed_live, preferred_element_type=F32).astype(BF16)
     return (mixed, new_state)
 
 

time: 136 us -> 119 us (0.88)
  local copies, waits for them, and re-layouts: 11.1 us -> 2.94 us
  Pallas kernels: 119 us -> 116 us
  other arithmetic: 2.97 us -> 0 us
  matrix products: 1.85 us -> 0 us
    unnamed x6 -> x2, local copies, waits for them, and re-layouts: 8.86 us -> 2.94 us
    pallas_call x1, Pallas kernels: 21.2 us -> 18.9 us  [local(): remote(functools.partial(attend_kernel, kv_size, tp_size), jax.ShapeDtype...]
    broadcast_in_dim x3 -> x0, local copies, waits for them, and re-layouts: 2.06 us -> none  [the longest x1 1.25 us: local(): jnp.broadcast_to(later_rescale_vector.reshape(1, -1), (8, block))]
    dot_general x1 -> x0, matrix products: 1.85 us -> none  [local(): mixed = jnp.dot(pick.T, mixed_live, preferred_element_type=F32).astype(BF16)]
    pallas_call x1, Pallas kernels: 45.1 us -> 43.3 us  [local(): remote(functools.partial(project_kernel, kv_size, tp_size), (jax.ShapeDty...]
where the time goes in v2:
time: 119 us
  Pallas kernels  116 us (97%)
  local copies, waits for them, and re-layouts  2.94 us (2%)
    pallas_call x1, Pallas kernels, local(): remote(functools.partial(mixer_kernel, kv_size, tp_size), jax.ShapeDtypeS...  48 us
    pallas_call x1, Pallas kernels, local(): remote(functools.partial(project_kernel, kv_size, tp_size), (jax.ShapeDty...  43.3 us
    pallas_call x1, Pallas kernels, local(): remote(functools.partial(attend_kernel, kv_size, tp_size), jax.ShapeDtype...  18.9 us
    pallas_call x1, Pallas kernels, local(): pl.pallas_call(functools.partial(recur_kernel, features), out_shape=(jax....  5.33 us
    unnamed x2, local copies, waits for them, and re-layouts  2.94 us

profile of v2, /device:TPU:0, one launch (start us, length us, event | category | flops | bytes accessed | tf_op | source)
XLA Modules:
  0.0 119.2 jit_solution(4889479448769075234)
XLA Ops:
  0.6 1.4 %copy.18.shrink_ref = f32[64,4]{1,0:T(8,128)} copy(f32[64,4]{0,1:T(4,128)} %param.25) | data formatting | bytes 2048 | tf_op args[9]
  2.0 43.3 %project.1 = (f32[4,64,512]{2,1,0:T(8,128)}, f32[64,128]{1,0:T(8,128)}) custom-call(bf16[512,128]{1,0:T(8,128)(2,1)} %x_ref.3, f32[1,512]{1,0:T(1,128)} %bitcast.12, bf16[512,512]{1,0:T(8,128)(2,1)} %w0.1, bf16[512,512]{1,0:T(8,128)(2,1)} %w1.1, bf16[512,512]{1,0:T(8,128)(2,1)} %w2.1, bf16[512,512]{1,0:T(8,128)(2,1)} %w3.1), custom_call_target="tpu_custom_call" | custom-call | tf_op jit(solution)/shard_map/project/pallas_call | solution.py:530
  45.3 5.3 %recur.1 = (bf16[64,512]{1,0:T(8,128)(2,1)}, f32[8,4,128,128]{3,2,1,0:T(8,128)}, f32[8,128]{1,0:T(8,128)}) custom-call(f32[4,64,512]{2,1,0:T(8,128)} %get-tuple-element.7.z_ref, f32[64,128]{1,0:T(8,128)} %get-tuple-element.8.sq_ref, f32[8,4,128,128]{3,2,1,0:T(8,128)} %state_ref.1, f32[1,512]{1,0:T(1,128)} %bitcast.13, f32[64,4]{1,0:T(8,128)} %copy.18.shrink_ref, ...), custom_call_target="tpu_custom_call" | custom-call | tf_op jit(solution)/shard_map/recur/pallas_call | solution.py:563
  50.7 18.9 %attend.1.x_ref = bf16[256,128]{1,0:T(8,128)(2,1)} custom-call(bf16[64,512]{1,0:T(8,128)(2,1)} %get-tuple-element.9.n_ref, s32[1,64]{1,0:T(1,128)} %bitcast.10, bf16[512,512]{1,0:T(8,128)(2,1)} %w_ref.1, bf16[512,128]{1,0:T(8,128)(2,1)} %x_ref.3), custom_call_target="tpu_custom_call" | custom-call | tf_op jit(solution)/shard_map/attend/pallas_call | solution.py:586
  69.6 48.0 %mixer.1 = bf16[512,128]{1,0:T(8,128)(2,1)} custom-call(bf16[256,128]{1,0:T(8,128)(2,1)} %attend.1.x_ref, f32[8,128]{1,0:T(8,128)} %get-tuple-element.10.gain_ref, s32[1,64]{1,0:T(1,128)} %bitcast.11, bf16[344,4096]{1,0:T(8,128)(2,1)} %bitcast.7, bf16[344,4096]{1,0:T(8,128)(2,1)} %bitcast.8, bf16[344,4096]{1,0:T(8,128)(2,1)} %wd_hbm.1), custom_call_target="tpu_custom_call" | custom-call | tf_op jit(solution)/shard_map/mixer/pallas_call | solution.py:621
  117.6 1.6 %copy.20 = bf16[512,128]{1,0:T(8,128)(2,1)} copy(bf16[512,128]{1,0:T(8,128)(2,1)} %mixer.1) | data formatting | bytes 262144
